TPU v7x, 32 devices: a whole 2x2x4 slice. The times are simulated.
32 devices in a mesh: kv: 8 (over z, y), tp: 4 (over x, core).
Axes of the slice: x: 2, y: 2, z: 4, core: 2. Of those that a mesh axis runs over, the one named last changes fastest.
Arguments:
- hidden_in: bfloat16 [16, 4096], P(None, ('kv', 'tp')), may hold values from -12 to 12
- attn_gain: float32 [4096], P('kv'), may hold values from 0.1 to 1.9
- query_weight: bfloat16 [4096, 4096], P('kv', 'tp'), may hold values from -0.09375 to 0.09375
- key_cache: bfloat16 [16, 8192, 8, 128], P(None, 'kv', 'tp'), may hold values from -600 to 600
- value_cache: bfloat16 [16, 8192, 8, 128], P(None, 'kv', 'tp'), may hold values from -6 to 6
- lambdas: float32 [32], P('tp'), may hold values from 0.3 to 0.8
- head_gain: float32 [128], replicated, may hold values from 0.1 to 1.9
- out_weight: bfloat16 [4096, 4096], P('tp', 'kv'), may hold values from -0.09375 to 0.09375
- mixer_gain: float32 [4096], P(('kv', 'tp')), may hold values from 0.1 to 1.9
- gate_weight: bfloat16 [4096, 11264], P('kv', 'tp'), may hold values from -0.09375 to 0.09375
- up_weight: bfloat16 [4096, 11264], P('kv', 'tp'), may hold values from -0.09375 to 0.09375
- down_weight: bfloat16 [11264, 4096], P('tp', 'kv'), may hold values from -0.0546875 to 0.0546875
Outputs:
- mixed: bfloat16 [16, 4096], P(None, ('kv', 'tp'))
All inputs are finite; a program needn't handle non-finite values.
Results may differ from a plain program's by a relative error of at most 0.017.
Values may be sent and summed in bfloat16 or wider, within the bound.
A program may use at most 64 MiB of HBM per device.

v0:
```python
import jax
import jax.numpy as jnp
from jax import lax
from jax.sharding import PartitionSpec as P

D = 4096
HEAD_DIM = 64
eps = 1e-06


def finish_heads(totals, weighted, lambdas, head_gain, kv_dev, group_size):
    head_means = weighted / totals[..., None]
    mixing = lambdas.reshape(kv_dev, group_size)
    attended = head_means[0] - mixing[None, :, :, None] * head_means[1]
    norm_inv = lax.rsqrt(jnp.mean(attended * attended, axis=-1, keepdims=True) + eps)
    head_out = (attended * norm_inv * head_gain).astype(jnp.bfloat16)
    return head_out.reshape(head_out.shape[0], kv_dev * group_size * 2 * HEAD_DIM)


def per_device(
    hidden_in,
    attn_gain,
    query_weight,
    key_cache,
    value_cache,
    lambdas,
    head_gain,
    out_weight,
    mixer_gain,
    gate_weight,
    up_weight,
    down_weight,
):
    batch_rows = hidden_in.shape[0]
    rows_block = lax.all_gather(hidden_in, "tp", axis=1, tiled=True)
    block_f = rows_block.astype(jnp.float32)
    gained = (block_f * attn_gain).astype(jnp.bfloat16)
    partial_value = jnp.dot(gained, query_weight, preferred_element_type=jnp.float32)
    own_cols = hidden_in.astype(jnp.float32)
    squares = lax.psum(jnp.sum(own_cols * own_cols, axis=1), ("kv", "tp"))
    query_full = lax.psum(partial_value, "kv")
    row_scale = lax.rsqrt(squares / D + eps)
    query_rows = (query_full * row_scale[:, None]).astype(jnp.bfloat16)
    positions = key_cache.shape[1]
    kv_dev = key_cache.shape[2]
    heads_dev = query_rows.shape[1] // (2 * HEAD_DIM)
    group_size = heads_dev // kv_dev
    query_heads = query_rows.reshape(batch_rows, kv_dev, group_size, 2, HEAD_DIM)
    key_rows = key_cache.reshape(batch_rows, positions, kv_dev, 2, HEAD_DIM)
    scores = jnp.einsum(
        "bkgcd,bpkcd->cbkgp", query_heads, key_rows, preferred_element_type=jnp.float32
    ) * HEAD_DIM ** (-0.5)
    maxima = jnp.max(scores, axis=-1)
    exponent = jnp.exp(scores - maxima[..., None])
    totals = jnp.sum(exponent, axis=-1)
    exp_weights = exponent.astype(jnp.bfloat16)
    weighted = jnp.einsum(
        "cbkgp,bpkv->cbkgv", exp_weights, value_cache, preferred_element_type=jnp.float32
    )
    parts_max, parts_tot, parts_acc = (
        lax.all_to_all(maxima[None], "kv", split_axis=2, concat_axis=0, tiled=True),
        lax.all_to_all(totals[None], "kv", split_axis=2, concat_axis=0, tiled=True),
        lax.all_to_all(weighted[None], "kv", split_axis=2, concat_axis=0, tiled=True),
    )
    top = jnp.max(parts_max, axis=0)
    factors = jnp.exp(parts_max - top[None])
    own_tot = jnp.sum(parts_tot * factors, axis=0)
    own_acc = jnp.sum(parts_acc * factors[..., None], axis=0)
    own_out = finish_heads(own_tot, own_acc, lambdas, head_gain, kv_dev, group_size)
    head_out = lax.all_gather(own_out, "kv", axis=0, tiled=True)
    projected = jnp.dot(head_out, out_weight, preferred_element_type=jnp.float32)
    attn_out = lax.psum_scatter(
        projected.astype(jnp.bfloat16), "tp", scatter_dimension=1, tiled=True
    ).astype(jnp.float32)
    after_attn = (hidden_in.astype(jnp.float32) + attn_out).astype(jnp.bfloat16)
    after_f = after_attn.astype(jnp.float32)
    squares_two = lax.psum(jnp.sum(after_f * after_f, axis=1), ("kv", "tp"))
    mixer_in = (after_f * lax.rsqrt(squares_two / D + eps)[:, None] * mixer_gain).astype(
        jnp.bfloat16
    )
    gathered = lax.all_gather(mixer_in, "tp", axis=1, tiled=True)
    gate_part = jnp.dot(gathered, gate_weight, preferred_element_type=jnp.float32)
    up_part = jnp.dot(gathered, up_weight, preferred_element_type=jnp.float32)
    gate_sum, up_sum = lax.psum((gate_part, up_part), "kv")
    hidden = (jax.nn.silu(gate_sum) * up_sum).astype(jnp.bfloat16)
    down_part = jnp.dot(hidden, down_weight, preferred_element_type=jnp.float32)
    mixer_out = lax.psum_scatter(
        down_part.astype(jnp.bfloat16), "tp", scatter_dimension=1, tiled=True
    ).astype(jnp.float32)
    return (after_f + mixer_out).astype(jnp.bfloat16)


def solution(mesh):
    in_specs = (
        P(None, ("kv", "tp")),
        P("kv"),
        P("kv", "tp"),
        P(None, "kv", "tp", None),
        P(None, "kv", "tp", None),
        P("tp"),
        P(),
        P("tp", "kv"),
        P(("kv", "tp")),
        P("kv", "tp"),
        P("kv", "tp"),
        P("tp", "kv"),
    )
    out_specs = P(None, ("kv", "tp"))
    return jax.shard_map(
        per_device, mesh=mesh, in_specs=in_specs, out_specs=out_specs, check_vma=False
    )
```

profile of v0, /device:TPU:0, one launch (start us, length us, event | category | flops | bytes accessed | tf_op | source)
XLA Modules:
  0.0 329.5 jit_solution(1171620726180046008)
XLA Ops:
  6.5 6.5 %all_gather.9 = bf16[16,512]{1,0:T(8,128)(2,1)S(1)} all-gather(bf16[16,128]{1,0:T(8,128)(2,1)} %param.12), channel_id=1, replica_groups=mesh['kv'=8,'tp'=4] {'tp'}, dimensions={1}, use_global_device_ids=true | all-gather | bytes 20480 | tf_op jit(solution)/shard_map/all_gather | solution.py:35
  13.0 0.8 fusion.17
  13.8 2.1 fusion.15
  16.0 41.0 %psum.36 = f32[16]{0:T(128)S(1)} all-reduce(f32[16]{0:T(128)S(1)} %fusion.17), channel_id=1, replica_groups=mesh['kv'=8,'tp'=4] {'kv','tp'}, use_global_device_ids=true, to_apply=%region_2.0 | all-reduce | flops 16 | bytes 128 | tf_op jit(solution)/shard_map/psum | solution.py:40
  57.0 21.2 %copy.33 = bf16[16,1024,2,128]{1,3,2,0:T(8,128)(2,1)} copy(bf16[16,1024,2,128]{3,2,1,0:T(2,128)(2,1)} %param.15) | data formatting | bytes 16777216 | tf_op args[3]
  78.2 9.0 %all-reduce.4.cloned.1.call-done = f32[16,1024]{1,0:T(8,128)} async-done(((f32[16,1024]{1,0:T(8,128)}), f32[16,1024]{1,0:T(8,128)}) %all-reduce.4.cloned.1.call-update) | async-done | bytes 65552 | tf_op jit(solution)/shard_map/psum | solution.py:41
  87.1 0.9 multiply_convert_fusion.2
  88.2 4.7 %fusion.28 = (f32[2,16,2,4]{3,2,1,0:T(2,128)S(1)}, f32[2,16,2,4,1024]{4,3,2,1,0:T(4,128)S(1)}) fusion(bf16[16,1024,2,2,64]{1,4,3,2,0:T(8,128)(2,1)} %bitcast.56, bf16[16,2,4,2,64]{4,3,2,1,0:T(2,128)(2,1)S(1)} %reshape.35), kind=kOutput, calls=%fused_computation.46 | convolution fusion | flops 34078464 | bytes 9470976 | tf_op jit(solution)/shard_map/bkgcd,bpkcd->cbkgp/dot_general | solution.py:50
  92.9 0.6 fusion.10
  93.5 0.6 copy.41
  94.1 4.5 %all-to-all-start.2 = ((f32[1,2,16,2,4]{4,3,1,0,2:T(2,128)}), f32[1,2,16,2,4]{4,3,1,0,2:T(2,128)S(1)}, u32[]{:S(2)}, u32[]{:S(2)}) async-start(f32[1,2,16,2,4]{4,3,1,0,2:T(2,128)} %copy.41), calls=%async_computation.2 | async-start | bytes 65536 | tf_op jit(solution)/shard_map/all_to_all | solution.py:62
  99.3 6.1 %all-to-all-done.2 = f32[1,2,16,2,4]{4,3,1,0,2:T(2,128)S(1)} async-done(((f32[1,2,16,2,4]{4,3,1,0,2:T(2,128)}), f32[1,2,16,2,4]{4,3,1,0,2:T(2,128)S(1)}, u32[]{:S(2)}, u32[]{:S(2)}) %all-to-all-start.2) | async-done | bytes 1056 | tf_op jit(solution)/shard_map/all_to_all | solution.py:62
  105.3 3.3 %all-to-all-start.1 = ((f32[1,2,16,2,4]{4,3,1,0,2:T(2,128)}), f32[1,2,16,2,4]{4,3,1,0,2:T(2,128)S(1)}, u32[]{:S(2)}, u32[]{:S(2)}) async-start(f32[1,2,16,2,4]{4,3,1,0,2:T(2,128)} %copy.39), calls=%async_computation.1 | async-start | bytes 65536 | tf_op jit(solution)/shard_map/all_to_all | solution.py:61
  108.7 5.5 %fusion.7 = f32[1,2,16,2,4,128]{5,4,1,3,0,2:T(4,128)} fusion(bf16[16,1024,2,128,1]{3,2,1,0,4:T(2,128)(2,1)} %bitcast.69, bf16[2,16,2,4,1024]{4,3,2,1,0:T(4,128)(2,1)S(1)} %get-tuple-element.10), kind=kOutput, calls=%fused_computation.5 | convolution fusion | flops 67108864 | bytes 9043968 | tf_op jit(solution)/shard_map/cbkgp,bpkv->cbkgv/dot_general | solution.py:57
  114.2 1.1 all-to-all-done.1
  115.3 4.8 %all-to-all-start = ((f32[1,2,16,2,4,128]{5,4,1,3,0,2:T(4,128)}), f32[1,2,16,2,4,128]{5,4,1,3,0,2:T(4,128)S(1)}, u32[]{:S(2)}, u32[]{:S(2)}) async-start(f32[1,2,16,2,4,128]{5,4,1,3,0,2:T(4,128)} %fusion.7), calls=%async_computation | async-start | bytes 262144 | tf_op jit(solution)/shard_map/all_to_all | solution.py:63
  120.4 7.1 %all-to-all-done = f32[1,2,16,2,4,128]{5,4,1,3,0,2:T(4,128)S(1)} async-done(((f32[1,2,16,2,4,128]{5,4,1,3,0,2:T(4,128)}), f32[1,2,16,2,4,128]{5,4,1,3,0,2:T(4,128)S(1)}, u32[]{:S(2)}, u32[]{:S(2)}) %all-to-all-start) | async-done | bytes 131104 | tf_op jit(solution)/shard_map/all_to_all | solution.py:63
  128.1 30.6 %all-gather = bf16[8,2,1024]{2,1,0:T(2,128)(2,1)S(1)} all-gather(bf16[1,2,1024]{2,1,0:T(2,128)(2,1)S(1)} %fusion.25), channel_id=1, replica_groups=mesh['kv'=8,'tp'=4] {'kv'}, dimensions={0}, use_global_device_ids=true | all-gather | bytes 36864 | tf_op jit(solution)/shard_map/all_gather | solution.py:70
  158.8 1.5 convolution_convert_fusion.1
  160.2 0.8 copy.47
  161.1 17.5 %reduce-scatter.7.cloned.1.call-done = bf16[128,16]{1,0:T(8,128)(2,1)} async-done(((bf16[512,16]{1,0:T(8,128)(2,1)}), bf16[128,16]{1,0:T(8,128)(2,1)}) %reduce-scatter.7.cloned.1.call-update) | async-done | bytes 4112
  178.6 0.8 copy.48
  179.5 39.3 %psum.37 = f32[16]{0:T(128)S(1)} all-reduce(f32[16]{0:T(128)S(1)} %fusion.19), channel_id=1, replica_groups=mesh['kv'=8,'tp'=4] {'kv','tp'}, use_global_device_ids=true, to_apply=%region_11.0 | all-reduce | flops 16 | bytes 128 | tf_op jit(solution)/shard_map/psum | solution.py:77
  218.9 5.6 %all_gather.11 = bf16[16,512]{1,0:T(8,128)(2,1)S(1)} all-gather(bf16[16,128]{1,0:T(8,128)(2,1)S(1)} %fusion.21), channel_id=1, replica_groups=mesh['kv'=8,'tp'=4] {'tp'}, dimensions={1}, use_global_device_ids=true | all-gather | bytes 20480 | tf_op jit(solution)/shard_map/all_gather | solution.py:81
  224.5 1.2 fusion.29
  225.6 1.2 fusion.30
  226.9 72.3 %all-reduce.6.cloned.1.call-done = (f32[16,2816]{1,0:T(8,128)}, f32[16,2816]{1,0:T(8,128)}) async-done(((f32[16,2816]{1,0:T(8,128)}, f32[16,2816]{1,0:T(8,128)}), (f32[16,2816]{1,0:T(8,128)}, f32[16,2816]{1,0:T(8,128)})) %all-reduce.6.cloned.1.call-update) | async-done | bytes 360464 | tf_op jit(solution)/shard_map/psum | solution.py:84
  299.2 2.5 convolution_convert_fusion
  301.7 0.7 copy.49
  302.5 19.1 %reduce-scatter.9.cloned.1.call-done = bf16[128,16]{1,0:T(8,128)(2,1)} async-done(((bf16[512,16]{1,0:T(8,128)(2,1)}), bf16[128,16]{1,0:T(8,128)(2,1)}) %reduce-scatter.9.cloned.1.call-update) | async-done | bytes 4112
  321.6 0.8 copy.50
  322.4 0.6 fusion.22
  (44 shorter events, 2.0 us)
Async XLA Ops:
  6.5 217.9 %copy-start = (bf16[512,2816]{1,0:T(8,128)(2,1)S(1)}, bf16[512,2816]{1,0:T(8,128)(2,1)}, u32[]{:S(2)}) copy-start(bf16[512,2816]{1,0:T(8,128)(2,1)} %param.21) | copy-start | bytes 8650756
  6.5 80.6 %all-reduce.4.cloned.1.call-start = ((), (), s32[]{:S(2)}) async-start(), calls=%async_computation.5 | async-start | bytes 131072 | tf_op jit(solution)/shard_map/psum | solution.py:41
  94.1 11.2 %all-to-all-start.2 = ((f32[1,2,16,2,4]{4,3,1,0,2:T(2,128)}), f32[1,2,16,2,4]{4,3,1,0,2:T(2,128)S(1)}, u32[]{:S(2)}, u32[]{:S(2)}) async-start(f32[1,2,16,2,4]{4,3,1,0,2:T(2,128)} %copy.41), calls=%async_computation.2 | async-start | bytes 65536 | tf_op jit(solution)/shard_map/all_to_all | solution.py:62
  105.3 10.0 %all-to-all-start.1 = ((f32[1,2,16,2,4]{4,3,1,0,2:T(2,128)}), f32[1,2,16,2,4]{4,3,1,0,2:T(2,128)S(1)}, u32[]{:S(2)}, u32[]{:S(2)}) async-start(f32[1,2,16,2,4]{4,3,1,0,2:T(2,128)} %copy.39), calls=%async_computation.1 | async-start | bytes 65536 | tf_op jit(solution)/shard_map/all_to_all | solution.py:61
  108.7 11.5 %copy-start.5 = (f32[8]{0:T(128)S(1)}, f32[8]{0:T(128)}, u32[]{:S(2)}) copy-start(f32[8]{0:T(128)} %param.17) | copy-start | bytes 100
  108.7 19.4 %copy-start.3 = (f32[128]{0:T(128)S(1)}, f32[128]{0:T(128)}, u32[]{:S(2)}) copy-start(f32[128]{0:T(128)} %param.18) | copy-start | bytes 1540
  108.7 70.7 %copy-start.2 = (bf16[16,128]{1,0:T(8,128)(2,1)S(1)}, bf16[16,128]{1,0:T(8,128)(2,1)}, u32[]{:S(2)}) copy-start(bf16[16,128]{1,0:T(8,128)(2,1)} %param.12) | copy-start | bytes 12292
  108.7 110.1 %copy-start.4 = (f32[128]{0:T(128)S(1)}, f32[128]{0:T(128)}, u32[]{:S(2)}) copy-start(f32[128]{0:T(128)} %param.20) | copy-start | bytes 1540
  115.3 12.2 %all-to-all-start = ((f32[1,2,16,2,4,128]{5,4,1,3,0,2:T(4,128)}), f32[1,2,16,2,4,128]{5,4,1,3,0,2:T(4,128)S(1)}, u32[]{:S(2)}, u32[]{:S(2)}) async-start(f32[1,2,16,2,4,128]{5,4,1,3,0,2:T(4,128)} %fusion.7), calls=%async_computation | async-start | bytes 262144 | tf_op jit(solution)/shard_map/all_to_all | solution.py:63
  120.1 58.4 %reduce-scatter.7.cloned.1.call-start = ((), (), s32[]{:S(2)}) async-start(), calls=%async_computation.6 | async-start | bytes 163840
  161.0 138.2 %all-reduce.6.cloned.1.call-start = ((), (), s32[]{:S(2)}) async-start(), calls=%async_computation.8 | async-start | bytes 720896 | tf_op jit(solution)/shard_map/psum | solution.py:84
  218.8 6.8 %copy-start.1 = (bf16[512,2816]{1,0:T(8,128)(2,1)S(1)}, bf16[512,2816]{1,0:T(8,128)(2,1)}, u32[]{:S(2)}) copy-start(bf16[512,2816]{1,0:T(8,128)(2,1)} %param.22) | copy-start | bytes 8650756
  226.8 94.8 %reduce-scatter.9.cloned.1.call-start = ((), (), s32[]{:S(2)}) async-start(), calls=%async_computation.7 | async-start | bytes 163840
Sparse Core Ops, SparseCore 0:
  16.1 71.0 all-reduce.3
  161.1 17.3 reduce-scatter.6
  226.9 72.2 all-reduce.5
  302.6 18.9 reduce-scatter.8
where the time goes:
time: 331 us; the launch traced here: 330 us
  waiting for transfers between devices  132 us (40%)
  blocking collectives  123 us (37%)
  local copies, waits for them, and re-layouts  26 us (8%)
  matrix products  18.6 us (6%)
  between operations  13.3 us (4%)
  starting transfers between devices  12.8 us (4%)
  other arithmetic  3.66 us (1%)
    psum x1, waiting for transfers between devices, per_device(): gate_sum, up_sum = lax.psum((gate_part, up_part), 'kv')  72.3 us
    psum x1, blocking collectives, per_device(): squares = lax.psum(jnp.sum(own_cols * own_cols, axis=1), ('kv', 'tp'))  41 us
    psum x1, blocking collectives, per_device(): squares_two = lax.psum(jnp.sum(after_f * after_f, axis=1), ('kv', 'tp'))  39.3 us
    unnamed x6, waiting for transfers between devices  36.7 us
    all_gather x1, blocking collectives, per_device(): head_out = lax.all_gather(own_out, 'kv', axis=0, tiled=True)  30.6 us
    unnamed x18, local copies, waits for them, and re-layouts  24.3 us
    psum x1, waiting for transfers between devices, per_device(): query_full = lax.psum(partial_value, 'kv')  8.99 us
    all_to_all x1, waiting for transfers between devices, per_device(): lax.all_to_all(weighted[None], 'kv', split_axis=2, concat_axis=0, tiled=T...  7.09 us
  transfers between devices with their start and end apart: 7, of which 7 were waited for; matrix products, arithmetic and copies ran while one was open for 8% of the time, Pallas kernels for 0%

commit v1 on v0

--- a/solution.py
+++ b/solution.py
@@ -74,7 +74,9 @@
     ).astype(jnp.float32)
     after_attn = (hidden_in.astype(jnp.float32) + attn_out).astype(jnp.bfloat16)
     after_f = after_attn.astype(jnp.float32)
-    squares_two = lax.psum(jnp.sum(after_f * after_f, axis=1), ("kv", "tp"))
+    block = jnp.sum(after_f * after_f, axis=1)
+    pieces = lax.all_gather(block, ("kv", "tp"), axis=0, tiled=False)
+    squares_two = pieces.sum(axis=0)
     mixer_in = (after_f * lax.rsqrt(squares_two / D + eps)[:, None] * mixer_gain).astype(
         jnp.bfloat16
     )

time: 331 us -> 331 us (level)
    psum x1 -> x0, blocking collectives: 39.3 us -> none  [per_device(): squares_two = lax.psum(jnp.sum(after_f * after_f, axis=1), ('kv', 'tp'))]
    unnamed x0 -> x1, blocking collectives: none -> 39.2 us
    unnamed x18 -> x20, local copies, waits for them, and re-layouts: 24.3 us -> 24.6 us
where the time goes in v1:
time: 331 us; the launch traced here: 330 us
  waiting for transfers between devices  132 us (40%)
  blocking collectives  123 us (37%)
  local copies, waits for them, and re-layouts  26.3 us (8%)
  matrix products  18.6 us (6%)
  between operations  13.3 us (4%)
  starting transfers between devices  12.8 us (4%)
  other arithmetic  3.69 us (1%)
    psum x1, waiting for transfers between devices, per_device(): gate_sum, up_sum = lax.psum((gate_part, up_part), 'kv')  72.3 us
    psum x1, blocking collectives, per_device(): squares = lax.psum(jnp.sum(own_cols * own_cols, axis=1), ('kv', 'tp'))  41 us
    unnamed x1, blocking collectives  39.2 us
    unnamed x6, waiting for transfers between devices  36.7 us
    all_gather x1, blocking collectives, per_device(): head_out = lax.all_gather(own_out, 'kv', axis=0, tiled=True)  30.6 us
    unnamed x20, local copies, waits for them, and re-layouts  24.6 us
    psum x1, waiting for transfers between devices, per_device(): query_full = lax.psum(partial_value, 'kv')  8.99 us
    all_to_all x1, waiting for transfers between devices, per_device(): lax.all_to_all(weighted[None], 'kv', split_axis=2, concat_axis=0, tiled=T...  7.09 us
  transfers between devices with their start and end apart: 7, of which 7 were waited for; matrix products, arithmetic and copies ran while one was open for 8% of the time, Pallas kernels for 0%

profile of v1, /device:TPU:0, one launch (start us, length us, event | category | flops | bytes accessed | tf_op | source)
XLA Modules:
  0.0 329.9 jit_solution(6588057418720872200)
XLA Ops:
  6.5 6.5 %all_gather.15 = bf16[16,512]{1,0:T(8,128)(2,1)S(1)} all-gather(bf16[16,128]{1,0:T(8,128)(2,1)} %param.12), channel_id=1, replica_groups=mesh['kv'=8,'tp'=4] {'tp'}, dimensions={1}, use_global_device_ids=true | all-gather | bytes 20480 | tf_op jit(solution)/shard_map/all_gather | solution.py:35
  13.0 0.8 fusion.17
  13.8 2.1 fusion.15
  16.0 41.0 %psum.29 = f32[16]{0:T(128)S(1)} all-reduce(f32[16]{0:T(128)S(1)} %fusion.17), channel_id=1, replica_groups=mesh['kv'=8,'tp'=4] {'kv','tp'}, use_global_device_ids=true, to_apply=%region_2.0 | all-reduce | flops 16 | bytes 128 | tf_op jit(solution)/shard_map/psum | solution.py:40
  57.0 21.2 %copy.33 = bf16[16,1024,2,128]{1,3,2,0:T(8,128)(2,1)} copy(bf16[16,1024,2,128]{3,2,1,0:T(2,128)(2,1)} %param.15) | data formatting | bytes 16777216 | tf_op args[3]
  78.2 9.0 %all-reduce.5.cloned.1.call-done = f32[16,1024]{1,0:T(8,128)} async-done(((f32[16,1024]{1,0:T(8,128)}), f32[16,1024]{1,0:T(8,128)}) %all-reduce.5.cloned.1.call-update) | async-done | bytes 65552 | tf_op jit(solution)/shard_map/psum | solution.py:41
  87.1 0.9 multiply_convert_fusion.2
  88.2 4.7 %fusion.28 = (f32[2,16,2,4]{3,2,1,0:T(2,128)S(1)}, f32[2,16,2,4,1024]{4,3,2,1,0:T(4,128)S(1)}) fusion(bf16[16,1024,2,2,64]{1,4,3,2,0:T(8,128)(2,1)} %bitcast.56, bf16[16,2,4,2,64]{4,3,2,1,0:T(2,128)(2,1)S(1)} %reshape.39), kind=kOutput, calls=%fused_computation.46 | convolution fusion | flops 34078464 | bytes 9470976 | tf_op jit(solution)/shard_map/bkgcd,bpkcd->cbkgp/dot_general | solution.py:50
  92.9 0.6 fusion.10
  93.5 0.6 copy.41
  94.1 4.5 %all-to-all-start.2 = ((f32[1,2,16,2,4]{4,3,1,0,2:T(2,128)}), f32[1,2,16,2,4]{4,3,1,0,2:T(2,128)S(1)}, u32[]{:S(2)}, u32[]{:S(2)}) async-start(f32[1,2,16,2,4]{4,3,1,0,2:T(2,128)} %copy.41), calls=%async_computation.2 | async-start | bytes 65536 | tf_op jit(solution)/shard_map/all_to_all | solution.py:62
  99.3 6.1 %all-to-all-done.2 = f32[1,2,16,2,4]{4,3,1,0,2:T(2,128)S(1)} async-done(((f32[1,2,16,2,4]{4,3,1,0,2:T(2,128)}), f32[1,2,16,2,4]{4,3,1,0,2:T(2,128)S(1)}, u32[]{:S(2)}, u32[]{:S(2)}) %all-to-all-start.2) | async-done | bytes 1056 | tf_op jit(solution)/shard_map/all_to_all | solution.py:62
  105.3 3.3 %all-to-all-start.1 = ((f32[1,2,16,2,4]{4,3,1,0,2:T(2,128)}), f32[1,2,16,2,4]{4,3,1,0,2:T(2,128)S(1)}, u32[]{:S(2)}, u32[]{:S(2)}) async-start(f32[1,2,16,2,4]{4,3,1,0,2:T(2,128)} %copy.39), calls=%async_computation.1 | async-start | bytes 65536 | tf_op jit(solution)/shard_map/all_to_all | solution.py:61
  108.7 5.5 %fusion.7 = f32[1,2,16,2,4,128]{5,4,1,3,0,2:T(4,128)} fusion(bf16[16,1024,2,128,1]{3,2,1,0,4:T(2,128)(2,1)} %bitcast.69, bf16[2,16,2,4,1024]{4,3,2,1,0:T(4,128)(2,1)S(1)} %get-tuple-element.10), kind=kOutput, calls=%fused_computation.5 | convolution fusion | flops 67108864 | bytes 9043968 | tf_op jit(solution)/shard_map/cbkgp,bpkv->cbkgv/dot_general | solution.py:57
  114.2 1.1 all-to-all-done.1
  115.3 4.8 %all-to-all-start = ((f32[1,2,16,2,4,128]{5,4,1,3,0,2:T(4,128)}), f32[1,2,16,2,4,128]{5,4,1,3,0,2:T(4,128)S(1)}, u32[]{:S(2)}, u32[]{:S(2)}) async-start(f32[1,2,16,2,4,128]{5,4,1,3,0,2:T(4,128)} %fusion.7), calls=%async_computation | async-start | bytes 262144 | tf_op jit(solution)/shard_map/all_to_all | solution.py:63
  120.4 7.1 %all-to-all-done = f32[1,2,16,2,4,128]{5,4,1,3,0,2:T(4,128)S(1)} async-done(((f32[1,2,16,2,4,128]{5,4,1,3,0,2:T(4,128)}), f32[1,2,16,2,4,128]{5,4,1,3,0,2:T(4,128)S(1)}, u32[]{:S(2)}, u32[]{:S(2)}) %all-to-all-start) | async-done | bytes 131104 | tf_op jit(solution)/shard_map/all_to_all | solution.py:63
  128.1 30.6 %all-gather.1 = bf16[8,2,1024]{2,1,0:T(2,128)(2,1)S(1)} all-gather(bf16[1,2,1024]{2,1,0:T(2,128)(2,1)S(1)} %fusion.25), channel_id=1, replica_groups=mesh['kv'=8,'tp'=4] {'kv'}, dimensions={0}, use_global_device_ids=true | all-gather | bytes 36864 | tf_op jit(solution)/shard_map/all_gather | solution.py:70
  158.8 1.5 convolution_convert_fusion.1
  160.2 0.8 copy.47
  161.1 17.5 %reduce-scatter.7.cloned.1.call-done = bf16[128,16]{1,0:T(8,128)(2,1)} async-done(((bf16[512,16]{1,0:T(8,128)(2,1)}), bf16[128,16]{1,0:T(8,128)(2,1)}) %reduce-scatter.7.cloned.1.call-update) | async-done | bytes 4112
  178.6 0.8 copy.48
  179.8 39.2 %all-reduce = f32[512]{0:T(512)S(1)} all-reduce(f32[512]{0:T(512)S(1)} %dynamic-update-slice), channel_id=2, replica_groups=mesh['kv'=8,'tp'=4] {'kv','tp'}, use_global_device_ids=true, to_apply=%add | all-reduce | flops 512 | bytes 4096
  219.2 5.6 %all_gather.19 = bf16[16,512]{1,0:T(8,128)(2,1)S(1)} all-gather(bf16[16,128]{1,0:T(8,128)(2,1)S(1)} %fusion.21), channel_id=1, replica_groups=mesh['kv'=8,'tp'=4] {'tp'}, dimensions={1}, use_global_device_ids=true | all-gather | bytes 20480 | tf_op jit(solution)/shard_map/all_gather | solution.py:83
  224.8 1.2 fusion.29
  226.0 1.2 fusion.30
  227.2 72.3 %all-reduce.7.cloned.1.call-done = (f32[16,2816]{1,0:T(8,128)}, f32[16,2816]{1,0:T(8,128)}) async-done(((f32[16,2816]{1,0:T(8,128)}, f32[16,2816]{1,0:T(8,128)}), (f32[16,2816]{1,0:T(8,128)}, f32[16,2816]{1,0:T(8,128)})) %all-reduce.7.cloned.1.call-update) | async-done | bytes 360464 | tf_op jit(solution)/shard_map/psum | solution.py:86
  299.5 2.5 convolution_convert_fusion
  302.0 0.7 copy.49
  302.8 19.1 %reduce-scatter.9.cloned.1.call-done = bf16[128,16]{1,0:T(8,128)(2,1)} async-done(((bf16[512,16]{1,0:T(8,128)(2,1)}), bf16[128,16]{1,0:T(8,128)(2,1)}) %reduce-scatter.9.cloned.1.call-update) | async-done | bytes 4112
  321.9 0.8 copy.50
  322.7 0.6 fusion.22
  (48 shorter events, 2.3 us)
Async XLA Ops:
  6.5 218.3 %copy-start = (bf16[512,2816]{1,0:T(8,128)(2,1)S(1)}, bf16[512,2816]{1,0:T(8,128)(2,1)}, u32[]{:S(2)}) copy-start(bf16[512,2816]{1,0:T(8,128)(2,1)} %param.21) | copy-start | bytes 8650756
  6.5 80.6 %all-reduce.5.cloned.1.call-start = ((), (), s32[]{:S(2)}) async-start(), calls=%async_computation.5 | async-start | bytes 131072 | tf_op jit(solution)/shard_map/psum | solution.py:41
  94.1 11.2 %all-to-all-start.2 = ((f32[1,2,16,2,4]{4,3,1,0,2:T(2,128)}), f32[1,2,16,2,4]{4,3,1,0,2:T(2,128)S(1)}, u32[]{:S(2)}, u32[]{:S(2)}) async-start(f32[1,2,16,2,4]{4,3,1,0,2:T(2,128)} %copy.41), calls=%async_computation.2 | async-start | bytes 65536 | tf_op jit(solution)/shard_map/all_to_all | solution.py:62
  105.3 10.0 %all-to-all-start.1 = ((f32[1,2,16,2,4]{4,3,1,0,2:T(2,128)}), f32[1,2,16,2,4]{4,3,1,0,2:T(2,128)S(1)}, u32[]{:S(2)}, u32[]{:S(2)}) async-start(f32[1,2,16,2,4]{4,3,1,0,2:T(2,128)} %copy.39), calls=%async_computation.1 | async-start | bytes 65536 | tf_op jit(solution)/shard_map/all_to_all | solution.py:61
  108.7 11.5 %copy-start.5 = (f32[8]{0:T(128)S(1)}, f32[8]{0:T(128)}, u32[]{:S(2)}) copy-start(f32[8]{0:T(128)} %param.17) | copy-start | bytes 100
  108.7 19.4 %copy-start.3 = (f32[128]{0:T(128)S(1)}, f32[128]{0:T(128)}, u32[]{:S(2)}) copy-start(f32[128]{0:T(128)} %param.18) | copy-start | bytes 1540
  108.7 70.7 %copy-start.2 = (bf16[16,128]{1,0:T(8,128)(2,1)S(1)}, bf16[16,128]{1,0:T(8,128)(2,1)}, u32[]{:S(2)}) copy-start(bf16[16,128]{1,0:T(8,128)(2,1)} %param.12) | copy-start | bytes 12292
  108.7 110.4 %copy-start.4 = (f32[128]{0:T(128)S(1)}, f32[128]{0:T(128)}, u32[]{:S(2)}) copy-start(f32[128]{0:T(128)} %param.20) | copy-start | bytes 1540
  115.3 12.2 %all-to-all-start = ((f32[1,2,16,2,4,128]{5,4,1,3,0,2:T(4,128)}), f32[1,2,16,2,4,128]{5,4,1,3,0,2:T(4,128)S(1)}, u32[]{:S(2)}, u32[]{:S(2)}) async-start(f32[1,2,16,2,4,128]{5,4,1,3,0,2:T(4,128)} %fusion.7), calls=%async_computation | async-start | bytes 262144 | tf_op jit(solution)/shard_map/all_to_all | solution.py:63
  120.1 58.4 %reduce-scatter.7.cloned.1.call-start = ((), (), s32[]{:S(2)}) async-start(), calls=%async_computation.6 | async-start | bytes 163840
  161.0 138.5 %all-reduce.7.cloned.1.call-start = ((), (), s32[]{:S(2)}) async-start(), calls=%async_computation.8 | async-start | bytes 720896 | tf_op jit(solution)/shard_map/psum | solution.py:86
  219.1 6.8 %copy-start.1 = (bf16[512,2816]{1,0:T(8,128)(2,1)S(1)}, bf16[512,2816]{1,0:T(8,128)(2,1)}, u32[]{:S(2)}) copy-start(bf16[512,2816]{1,0:T(8,128)(2,1)} %param.22) | copy-start | bytes 8650756
  227.1 94.8 %reduce-scatter.9.cloned.1.call-start = ((), (), s32[]{:S(2)}) async-start(), calls=%async_computation.7 | async-start | bytes 163840
Sparse Core Ops, SparseCore 0:
  16.1 71.0 all-reduce.4
  161.1 17.3 reduce-scatter.6
  227.3 72.2 all-reduce.6
  302.9 18.9 reduce-scatter.8
